TPU v7x, 32 devices: a whole 2x2x4 slice. The times are simulated.
32 devices in a mesh: grp: 2 (over x), row: 4 (over z), col: 4 (over y, core).
Axes of the slice: x: 2, y: 2, z: 4, core: 2. Of those that a mesh axis runs over, the one named last changes fastest.
Arguments:
- gate_in: bfloat16 [8, 512, 1024], P(('grp', 'row'), 'col'), parts along dimension 0, may hold values from -6 to 6
- mult_in: bfloat16 [8, 512, 1024], P(('grp', 'row'), 'col'), parts along dimension 0, may hold values from -6 to 6
- value_in: bfloat16 [8, 512, 1024], P(('grp', 'row'), 'col'), parts along dimension 0, may hold values from -6 to 6
- taps_gate: float32 [3, 1024], replicated, may hold values from -3.5 to 3.5
- taps_mult: float32 [3, 1024], replicated, may hold values from -3.5 to 3.5
- taps_value: float32 [3, 1024], replicated, may hold values from -3.5 to 3.5
- filter_first: float32 [33, 128], replicated, may hold values from -3 to 3
- filter_second: float32 [128, 128], replicated, may hold values from -1 to 1
- filter_ahead: float32 [128, 1024], replicated, may hold values from -0.5 to 0.5
- filter_behind: float32 [128, 1024], replicated, may hold values from -0.5 to 0.5
- filter_decay: float32 [1024], replicated, may hold values from 0.05 to 17.033333
- skip_gain: float32 [1024], replicated, may hold values from -5 to 5
- out_weight: bfloat16 [1024, 2048], replicated, may hold values from -0.1875 to 0.1875
Outputs:
- mixed: bfloat16 [8, 512, 2048], P(('grp', 'row'), 'col'), parts along dimension 0
There are 2 independent parts, one for each index of `grp`. A program takes and returns all parts, laid end to end along the dimension named above; an argument that names none is the same for every part. Nothing has to cross between parts.
All inputs are finite; a program needn't handle non-finite values.
Results may differ from a plain program's by a relative error of at most 0.0049.
Values may be sent and summed in bfloat16 or wider, within the bound.
A program may use at most 64 MiB of HBM per device.

v0:
```python
import math

import jax
import jax.numpy as jnp
from jax import lax
from jax.sharding import PartitionSpec as P

highest = lax.Precision.HIGHEST


def padded_2(shard, sides, width):
    for axis, dim in sides:
        size, length = (lax.axis_size(axis), shard.shape[dim])
        up = [(i, (i + 1) % size) for i in range(size - 1)]
        down = [(j, i) for i, j in up]
        last = lax.slice_in_dim(shard, length - width, length, axis=dim)
        leading = lax.slice_in_dim(shard, 0, width, axis=dim)
        before = lax.ppermute(last, axis, up)
        after = lax.ppermute(leading, axis, down)
        shard = jnp.concatenate([before, shard, after], axis=dim)
    return shard


def filter_hidden(mirror, seq_len, filter_first, filter_second):
    tau_values = mirror.astype(jnp.float32) / (seq_len - 1)
    omega_pos = 2.0 * math.pi / seq_len * mirror.astype(jnp.float32)
    band_count = (filter_first.shape[0] - 1) // 2
    band_values = jnp.linspace(0.0001, band_count - 1, band_count, dtype=jnp.float32)
    angles = omega_pos[:, None] * band_values[None, :]
    features = jnp.concatenate([tau_values[:, None], jnp.cos(angles), -jnp.sin(angles)], axis=1)
    hidden = jnp.sin(jnp.dot(features, filter_first, precision=highest))
    hidden = jnp.sin(jnp.dot(hidden, filter_second, precision=highest))
    return (hidden, tau_values)


def side_values(hidden, tau_values, side_weight, decay_rates):
    values = jnp.einsum("pf,fh->hp", hidden, side_weight, precision=highest)
    return values * jnp.exp(-decay_rates[:, None] * tau_values[None, :])


def angle_table(row_count, column_count, period):
    products = (
        lax.iota(jnp.int32, row_count)[:, None]
        * lax.iota(jnp.int32, column_count)[None, :]
        % period
    )
    angle = products.astype(jnp.float32) * (2.0 * math.pi / period)
    return (jnp.cos(angle), jnp.sin(angle))


def swap_halves(stacked, width):
    return jnp.concatenate([stacked[..., width:], stacked[..., :width]], axis=-1)


def forward(values, first_table, twist_even, twist_odd, second_block):
    channels, _, width = values.shape
    first = jnp.einsum("sfa,cab->cfsb", first_table, values, precision=highest)
    first = first.reshape(channels, first_table.shape[1], 2 * width)
    turned = first * twist_even + swap_halves(first, width) * twist_odd
    return jnp.einsum("cfk,kl->cfl", turned, second_block, precision=highest)


def inverse(spectrum, last_table, twist_even, twist_odd, second_block, span_len):
    channels, freq_rows, double_width = spectrum.shape
    width = double_width // 2
    back = jnp.einsum("cfk,kl->cfl", spectrum, second_block, precision=highest)
    turned = back * twist_even + swap_halves(back, width) * twist_odd
    turned = turned.reshape(channels, freq_rows, 2, width)
    result = jnp.einsum("asf,cfsb->cab", last_table, turned, precision=highest)
    return result / span_len


def body(
    gate_in,
    mult_in,
    value_in,
    taps_gate,
    taps_mult,
    taps_value,
    filter_first,
    filter_second,
    filter_ahead,
    filter_behind,
    filter_decay,
    skip_gain,
    out_weight,
):
    col_count = lax.axis_size("col")
    col_index = lax.axis_index("col")
    tok_rows = gate_in.shape[1]
    seq_len = tok_rows * col_count
    span_len = 2 * seq_len
    group_size = filter_ahead.shape[1] // col_count
    stacked = jnp.stack([gate_in[0], mult_in[0], value_in[0]])
    padded = padded_2(stacked, (("col", 1),), 1).astype(jnp.float32)
    all_taps = jnp.stack([taps_gate, taps_mult, taps_value])
    shorted = jnp.zeros(stacked.shape, jnp.float32)
    for offset in range(all_taps.shape[1]):
        shorted = shorted + all_taps[:, offset][:, None, :] * padded[:, offset : offset + tok_rows]
    gate_part = shorted[0]
    product = shorted[2] * shorted[1]
    spread = lax.all_to_all(product.T, "col", split_axis=0, concat_axis=1, tiled=True)
    first_channel = col_index * group_size
    own_rates = lax.dynamic_slice_in_dim(filter_decay, first_channel, group_size)
    mirror = lax.iota(jnp.int32, seq_len)
    hidden, tau_values = filter_hidden(mirror, seq_len, filter_first, filter_second)
    ahead_vals = side_values(
        hidden,
        tau_values,
        lax.dynamic_slice_in_dim(filter_ahead, first_channel, group_size, 1),
        own_rates,
    )
    behind_vals = side_values(
        hidden,
        tau_values,
        lax.dynamic_slice_in_dim(filter_behind, first_channel, group_size, 1),
        own_rates,
    )
    kernel = jnp.concatenate(
        [ahead_vals, jnp.zeros((group_size, 1), jnp.float32), jnp.flip(behind_vals[:, 1:], axis=1)],
        axis=1,
    )
    kernel = kernel * lax.rsqrt(jnp.sum(kernel * kernel, axis=1, keepdims=True) + 1e-06)
    factor = 128
    half_rows = factor // 2
    width_second = span_len // factor
    first_cos, first_sin = angle_table(factor, factor, factor)
    twist_cos, twist_sin = angle_table(factor, width_second, span_len)
    second_cos, second_sin = angle_table(width_second, width_second, width_second)
    first_table = jnp.stack([first_cos, -first_sin])
    last_table = jnp.stack([first_cos[:half_rows], -first_sin[:half_rows]], axis=1)
    twist_even = jnp.concatenate([twist_cos, twist_cos], axis=1)
    twist_ahead = jnp.concatenate([twist_sin, -twist_sin], axis=1)
    twist_back = jnp.concatenate([-twist_sin, twist_sin], axis=1)
    block_ahead = jnp.concatenate(
        [
            jnp.concatenate([second_cos, -second_sin], axis=1),
            jnp.concatenate([second_sin, second_cos], axis=1),
        ],
        axis=0,
    )
    block_back = jnp.concatenate(
        [
            jnp.concatenate([second_cos, second_sin], axis=1),
            jnp.concatenate([-second_sin, second_cos], axis=1),
        ],
        axis=0,
    )
    kernel_spec = forward(
        kernel.reshape(group_size, factor, width_second),
        first_table,
        twist_even,
        twist_ahead,
        block_ahead,
    )
    data_spec = forward(
        spread.reshape(group_size, half_rows, width_second),
        first_table[:, :, :half_rows],
        twist_even,
        twist_ahead,
        block_ahead,
    )
    data_re = data_spec[..., :width_second]
    data_im = data_spec[..., width_second:]
    kernel_re = kernel_spec[..., :width_second]
    kernel_im = kernel_spec[..., width_second:]
    joined = jnp.concatenate(
        [data_re * kernel_re - data_im * kernel_im, data_re * kernel_im + data_im * kernel_re],
        axis=-1,
    )
    convolved = inverse(joined, last_table, twist_even, twist_back, block_back, span_len).reshape(
        group_size, seq_len
    )
    returned = lax.all_to_all(convolved, "col", split_axis=1, concat_axis=0, tiled=True)
    mixed_rows = ((returned.T + skip_gain * product) * gate_part).astype(jnp.bfloat16)
    return jnp.dot(mixed_rows, out_weight, preferred_element_type=jnp.float32).astype(jnp.bfloat16)[
        None
    ]


def solution(mesh):
    in_specs = (
        P(("grp", "row"), "col", None),
        P(("grp", "row"), "col", None),
        P(("grp", "row"), "col", None),
        P(),
        P(),
        P(),
        P(),
        P(),
        P(),
        P(),
        P(),
        P(),
        P(),
    )
    out_specs = P(("grp", "row"), "col", None)
    return jax.shard_map(body, mesh=mesh, in_specs=in_specs, out_specs=out_specs, check_vma=False)
```

profile of v0, /device:TPU:0, one launch (start us, length us, event | category | flops | bytes accessed | tf_op | source)
XLA Modules:
  0.0 80.0 jit_solution(17331171744776615139)
XLA Ops:
  0.0 1.2 %copy.37 = bf16[1,128,1024]{1,2,0:T(8,128)(2,1)S(1)} copy(bf16[1,128,1024]{2,1,0:T(8,128)(2,1)} %param.13) | data formatting | bytes 524288 | tf_op args[0]
  1.2 1.2 %copy.38 = bf16[1,128,1024]{1,2,0:T(8,128)(2,1)S(1)} copy(bf16[1,128,1024]{2,1,0:T(8,128)(2,1)} %param.14) | data formatting | bytes 524288 | tf_op args[1]
  2.4 1.2 %copy.39 = bf16[1,128,1024]{1,2,0:T(8,128)(2,1)S(1)} copy(bf16[1,128,1024]{2,1,0:T(8,128)(2,1)} %param.15) | data formatting | bytes 524288 | tf_op args[2]
  3.7 0.0 copy-start.6
  3.7 0.7 copy-done.6
  4.4 0.1 pad_maximum_fusion.1
  4.5 0.3 fusion.116
  4.8 0.4 copy.40
  5.2 3.0 %collective-permute-start = (bf16[3,1,1024]{2,0,1:T(4,128)(2,1)S(1)}, bf16[3,1,1024]{2,0,1:T(4,128)(2,1)}, u32[]{:S(2)}, u32[]{:S(2)}) collective-permute-start(bf16[3,1,1024]{2,0,1:T(4,128)(2,1)S(1)} %copy.40), channel_id=1, source_target_pairs={{0,1},{1,2},{2,3},{4,5},{5,6},{6,7},{8,9},{9,10},{10,11},{12,13},{... | collective-permute-start | bytes 18440 | tf_op jit(solution)/shard_map/ppermute | solution.py:18
  8.1 1.0 %copy.41 = bf16[3,1,1024]{2,0,1:T(4,128)(2,1)} copy(bf16[3,1,1024]{1,2,0:T(8,128)(2,1)S(1)} %get-tuple-element.16) | data formatting | bytes 12288 | tf_op jit(solution)/shard_map/slice | solution.py:17
  9.1 1.3 %collective-permute-start.1 = (bf16[3,1,1024]{2,0,1:T(4,128)(2,1)}, bf16[3,1,1024]{2,0,1:T(4,128)(2,1)}, u32[]{:S(2)}, u32[]{:S(2)}) collective-permute-start(bf16[3,1,1024]{2,0,1:T(4,128)(2,1)} %copy.41), channel_id=1, source_target_pairs={{1,0},{2,1},{3,2},{5,4},{6,5},{7,6},{9,8},{10,9},{11,10},{13,12},{... | collective-permute-start | bytes 18440 | tf_op jit(solution)/shard_map/ppermute | solution.py:19
  10.5 0.3 sine_negate_fusion
  10.7 0.1 fusion.98
  10.8 0.7 fusion.96
  11.5 0.1 fusion.99
  11.6 0.1 pad_maximum_fusion.15
  11.6 0.2 multiply_cosine_fusion
  11.8 1.3 %convolution_sine_fusion.1 = f32[512,128]{1,0:T(8,128)S(1)} fusion(f32[33,128]{1,0:T(8,128)S(1)} %copy-done.16, f32[512,16]{0,1:T(8,128)S(1)} %get-tuple-element.25, f32[512,16]{0,1:T(8,128)S(1)} %get-tuple-element.24, f32[512,1]{0,1:T(1,128)S(1)} %convert_multiply_fusion.2), kind=kOutput, calls=%fused_computation.40 | convolution fusion | flops 25986048 | bytes 346624 | tf_op jit(solution)/shard_map/dot_general | solution.py:31
  13.2 1.2 %convolution_sine_fusion = f32[512,128]{1,0:T(8,128)S(1)} fusion(f32[512,128]{1,0:T(8,128)S(1)} %convolution_sine_fusion.1, f32[128,128]{1,0:T(8,128)S(1)} %copy-done.12), kind=kOutput, calls=%fused_computation.39 | convolution fusion | flops 100663296 | bytes 589824 | tf_op jit(solution)/shard_map/dot_general | solution.py:32
  14.4 0.8 dynamic-slice_negate_fusion
  15.1 0.6 fusion.48
  15.8 0.1 multiply_exponential_fusion
  15.9 0.3 slice_multiply_fusion.3
  16.3 0.8 reverse
  17.0 0.2 slice.164
  17.2 1.6 %convolution_multiply_fusion = f32[256,512]{1,0:T(8,128)S(1)} fusion(f32[512,128]{1,0:T(8,128)S(1)} %convolution_sine_fusion, f32[512]{0:T(512)S(1)} %convert_multiply_fusion, f32[256]{0:T(256)S(1)} %dynamic-slice_negate_fusion, f32[128,1024]{1,0:T(8,128)} %param.21, s32[]{:T(128)S(6)} %select_n.68), kind=kOutput, calls=%fused_computation.38 | convolution fusion | flops 201588736 | bytes 920580 | tf_op jit(solution)/shard_map/pf,fh->hp/dot_general | solution.py:37
  18.8 0.3 multiply_reduce_fusion
  19.1 0.3 copy.47
  19.5 0.1 fusion.36
  19.5 1.8 %convolution_bitcast_fusion = f32[256,128,2,8]{1,0,2,3:T(8,128)S(1)} fusion(f32[256,128,8,1]{0,2,1,3:T(8,128)S(1)} %fusion.36, f32[1,128,128]{1,2,0:T(8,128)S(1)} %get-tuple-element.28, f32[1,128,128]{1,2,0:T(8,128)S(1)} %get-tuple-element.29), kind=kOutput, calls=%fused_computation.27 | convolution fusion | flops 805339136 | bytes 3276800 | tf_op jit(solution)/shard_map/sfa,cab->cfsb/dot_general | solution.py:57
  21.4 1.2 %copy.80 = f32[256,128,2,8]{1,3,2,0:T(8,128)S(1)} copy(f32[256,128,2,8]{1,0,2,3:T(8,128)S(1)} %convolution_bitcast_fusion) | data formatting | bytes 4194304 | tf_op jit(solution)/shard_map/sfa,cab->cfsb/transpose | solution.py:57
  22.6 0.0 copy-start.17
  22.6 0.0 copy-start.18
  22.7 1.5 %fusion.115 = (f32[256,128,8]{1,2,0:T(8,128)}, f32[256,128,8]{1,2,0:T(8,128)}) fusion(f32[256,128,16]{1,2,0:T(8,128)S(1)} %bitcast.107), kind=kLoop, calls=%fused_computation.171 | loop fusion | bytes 4194304 | tf_op jit(solution)/shard_map/slice | solution.py:52
  24.1 0.8 cosine_bitcast_fusion
  24.9 0.6 pad_maximum_fusion.14
  25.5 0.6 copy_bitcast_fusion.2
  26.2 0.6 copy.82
  26.8 1.1 %copy.42 = bf16[3,1,1024]{1,2,0:T(8,128)(2,1)S(1)} copy(bf16[3,1,1024]{2,0,1:T(4,128)(2,1)} %collective-permute-done) | data formatting | bytes 12288 | tf_op jit(solution)/shard_map/ppermute | solution.py:18
  27.9 1.9 %copy.43 = bf16[3,1,1024]{1,2,0:T(8,128)(2,1)} copy(bf16[3,1,1024]{2,0,1:T(4,128)(2,1)} %collective-permute-done.1) | data formatting | bytes 12288 | tf_op jit(solution)/shard_map/ppermute | solution.py:19
  29.8 2.2 %maximum_convert_fusion = f32[3,130,1024]{1,2,0:T(8,128)S(1)} fusion(bf16[3,1,1024]{1,2,0:T(8,128)(2,1)} %copy.43, bf16[1,128,1024]{1,2,0:T(8,128)(2,1)} %copy-done.6, bf16[1,128,1024]{1,2,0:T(8,128)(2,1)} %copy-done.5, bf16[1,128,1024]{1,2,0:T(8,128)(2,1)} %copy-done.4, bf16[3,1,1024]{1,2,0:T(8,128)(2,1)S(1)} %copy.42), kind=kLoop, calls=%fused_computation.34 | loop fusion | flops 3993600 | bytes 2396160 | tf_op jit(solution)/shard_map/convert_element_type | solution.py:95
  32.1 2.3 %fusion.24 = f32[3,128,1024]{1,2,0:T(8,128)S(1)} fusion(f32[3,130,1024]{1,2,0:T(8,128)S(1)} %maximum_convert_fusion, f32[3,1024]{1,0:T(4,128)S(1)} %copy-done.9, f32[3,1024]{1,0:T(4,128)S(1)} %copy-done.10, f32[3,1024]{1,0:T(4,128)S(1)} %bitcast.114), kind=kLoop, calls=%fused_computation.30 | loop fusion | flops 1966080 | bytes 6328320 | tf_op jit(solution)/shard_map/add | solution.py:99
  34.4 1.1 %copy-done.1 = f32[3,128,1024]{1,2,0:T(8,128)} copy-done((f32[3,128,1024]{1,2,0:T(8,128)}, f32[3,128,1024]{1,2,0:T(8,128)S(1)}, u32[]{:S(2)}) %copy-start.1) | copy-done | bytes 1572888
  35.6 0.8 %slice_multiply_fusion.4 = f32[1,128,1024]{1,2,0:T(8,128)} fusion(f32[3,128,1024]{1,2,0:T(8,128)S(1)} %fusion.24), kind=kLoop, calls=%fused_computation.59 | loop fusion | flops 131072 | bytes 1572864 | tf_op jit(solution)/shard_map/mul | solution.py:101
  36.4 5.6 %all-to-all-start = ((f32[4,256,128]{2,1,0:T(8,128)}), f32[4,256,128]{2,1,0:T(8,128)S(1)}, u32[]{:S(2)}, u32[]{:S(2)}) async-start(f32[4,256,128]{2,1,0:T(8,128)} %bitcast.5), calls=%async_computation | async-start | bytes 1048576 | tf_op jit(solution)/shard_map/all_to_all | solution.py:102
  42.0 0.1 fusion.101
  42.0 6.1 %fusion.7 = f32[256,128,16]{1,2,0:T(8,128)} fusion(f32[256,128,8]{1,2,0:T(8,128)} %get-tuple-element.14, f32[256,128,8]{1,2,0:T(8,128)} %get-tuple-element.13, f32[128,16]{0,1:T(8,128)S(1)} %get-tuple-element.23, f32[128,16]{0,1:T(8,128)S(1)} %pad_maximum_fusion.12, f32[8,8]{0,1:T(8,128)S(1)} %copy-done.14, f32[8,8]{0,1:T(8,128)S(1)} %copy-done.13, ...), kind=kOutput, calls=%fused_computation.9 | convolution fusion | flops 102761216 | bytes 6308608 | tf_op jit(solution)/shard_map/cfk,kl->cfl/dot_general | solution.py:60
  48.1 2.7 %all-to-all-done = f32[4,256,128]{2,1,0:T(8,128)S(1)} async-done(((f32[4,256,128]{2,1,0:T(8,128)}), f32[4,256,128]{2,1,0:T(8,128)S(1)}, u32[]{:S(2)}, u32[]{:S(2)}) %all-to-all-start) | async-done | bytes 524320 | tf_op jit(solution)/shard_map/all_to_all | solution.py:102
  50.8 0.2 copy.44
  51.0 1.9 %convolution_bitcast_fusion.1 = f32[256,128,2,8]{1,0,2,3:T(8,128)S(1)} fusion(f32[256,64,8,1]{0,2,1,3:T(8,128)S(1)} %bitcast.113, f32[1,128,128]{1,2,0:T(8,128)S(1)} %get-tuple-element.29, f32[1,128,128]{1,2,0:T(8,128)S(1)} %get-tuple-element.28), kind=kOutput, calls=%fused_computation.28 | convolution fusion | flops 402669568 | bytes 2752512 | tf_op jit(solution)/shard_map/sfa,cab->cfsb/dot_general | solution.py:57
  52.9 1.2 %copy.81 = f32[256,128,2,8]{1,3,2,0:T(8,128)S(1)} copy(f32[256,128,2,8]{1,0,2,3:T(8,128)S(1)} %convolution_bitcast_fusion.1) | data formatting | bytes 4194304 | tf_op jit(solution)/shard_map/sfa,cab->cfsb/transpose | solution.py:57
  54.1 0.1 fusion.114
  54.2 3.1 %fusion.2 = f32[256,128,16]{1,2,0:T(8,128)S(1)} fusion(f32[256,128,8]{1,2,0:T(8,128)S(1)} %get-tuple-element.12, f32[256,128,8]{1,2,0:T(8,128)S(1)} %get-tuple-element.11, f32[128,16]{0,1:T(8,128)S(1)} %get-tuple-element.23, f32[128,16]{0,1:T(8,128)S(1)} %pad_maximum_fusion.12, f32[8,8]{0,1:T(8,128)S(1)} %copy-done.14, f32[8,8]{0,1:T(8,128)S(1)} %copy-done.13, ...), kind=kOutput, calls=%fused_computation.4 | convolution fusion | flops 102761216 | bytes 6308608 | tf_op jit(solution)/shard_map/cfk,kl->cfl/dot_general | solution.py:60
  57.4 0.2 multiply_subtract_fusion
  57.6 2.1 %fusion.11 = f32[256,128,16]{1,2,0:T(8,128)S(1)} fusion(f32[256,128,8]{1,2,0:T(8,128)S(1)} %get-tuple-element.8, f32[256,128,8]{1,2,0:T(8,128)S(1)} %get-tuple-element.7, f32[8,8]{0,1:T(8,128)S(1)} %copy-done.14, f32[8,8]{0,1:T(8,128)S(1)} %fusion.101, f32[8,8]{0,1:T(8,128)S(1)} %copy-done.13), kind=kOutput, calls=%fused_computation.12 | convolution fusion | flops 101188352 | bytes 4195072 | tf_op jit(solution)/shard_map/cfk,kl->cfl/dot_general | solution.py:66
  59.8 0.1 fusion.113
  59.9 0.6 copy-done.7
  60.5 0.0 copy-done.8
  60.5 1.8 %fusion.32 = f32[256,64,8]{1,2,0:T(8,128)S(1)} fusion(f32[256,128,8]{1,2,0:T(8,128)S(1)} %get-tuple-element.10, f32[256,128,8]{1,2,0:T(8,128)S(1)} %get-tuple-element.9, f32[256,128,16]{1,2,0:T(8,128)S(1)} %fusion.11, f32[128,16]{0,1:T(8,128)S(1)} %copy-done.15, f32[128,16]{0,1:T(8,128)S(1)} %pad_maximum_fusion.12, f32[64,1,128]{2,0,1:T(8,128)S(1)} %copy-done.8, ...), kind=kOutput, calls=%fused_computation.37 | convolution fusion | flops 404897792 | bytes 4800512 | tf_op jit(solution)/shard_map/asf,cfsb->cab/dot_general | solution.py:69
  62.4 1.2 %copy.51 = f32[256,64,8]{0,2,1:T(8,128)} copy(f32[256,64,8]{1,2,0:T(8,128)S(1)} %fusion.32) | data formatting | bytes 1048576 | tf_op jit(solution)/shard_map/div | solution.py:70
  63.6 12.3 %all_to_all.35 = f32[256,4,128]{0,2,1:T(8,128)S(1)} all-to-all(f32[256,4,128]{0,2,1:T(8,128)} %bitcast.110), channel_id=1, replica_groups=mesh['grp'=2,'row'=4,'col'=4] {'col'}, dimensions={1} | all-to-all | bytes 1048576 | tf_op jit(solution)/shard_map/all_to_all | solution.py:174
  75.8 0.2 copy.52
  76.1 0.2 fusion.44
  76.3 3.7 %fusion = bf16[1,128,2048]{2,1,0:T(8,128)(2,1)} fusion(bf16[128,1024]{0,1:T(8,128)(2,1)S(1)} %fusion.44, bf16[1024,2048]{1,0:T(8,128)(2,1)} %param.25), kind=kOutput, calls=%fused_computation.1 | convolution fusion | flops 537133056 | bytes 4980736 | tf_op jit(solution)/shard_map/dot_general | solution.py:176
  (46 shorter events, 0.2 us)
Async XLA Ops:
  0.0 15.1 %copy-start = (f32[128,1024]{1,0:T(8,128)S(1)}, f32[128,1024]{1,0:T(8,128)}, u32[]{:S(2)}) copy-start(f32[128,1024]{1,0:T(8,128)} %param.22) | copy-start | bytes 1572868
  1.2 2.5 %copy-start.4 = (bf16[1,128,1024]{1,2,0:T(8,128)(2,1)}, bf16[1,128,1024]{1,2,0:T(8,128)(2,1)S(1)}, u32[]{:S(2)}) copy-start(bf16[1,128,1024]{1,2,0:T(8,128)(2,1)S(1)} %copy.37) | copy-start | bytes 786436
  2.4 1.2 %copy-start.5 = (bf16[1,128,1024]{1,2,0:T(8,128)(2,1)}, bf16[1,128,1024]{1,2,0:T(8,128)(2,1)S(1)}, u32[]{:S(2)}) copy-start(bf16[1,128,1024]{1,2,0:T(8,128)(2,1)S(1)} %copy.38) | copy-start | bytes 786436
  3.7 0.7 copy-start.6
  4.5 7.4 %copy-start.16 = (f32[33,128]{1,0:T(8,128)S(1)}, f32[33,128]{1,0:T(8,128)}, u32[]{:S(2)}) copy-start(f32[33,128]{1,0:T(8,128)} %param.19) | copy-start | bytes 50692
  4.5 8.7 %copy-start.12 = (f32[128,128]{1,0:T(8,128)S(1)}, f32[128,128]{1,0:T(8,128)}, u32[]{:S(2)}) copy-start(f32[128,128]{1,0:T(8,128)} %param.20) | copy-start | bytes 196612
  5.2 21.6 %collective-permute-start = (bf16[3,1,1024]{2,0,1:T(4,128)(2,1)S(1)}, bf16[3,1,1024]{2,0,1:T(4,128)(2,1)}, u32[]{:S(2)}, u32[]{:S(2)}) collective-permute-start(bf16[3,1,1024]{2,0,1:T(4,128)(2,1)S(1)} %copy.40), channel_id=1, source_target_pairs={{0,1},{1,2},{2,3},{4,5},{5,6},{6,7},{8,9},{9,10},{10,11},{12,13},{... | collective-permute-start | bytes 18440 | tf_op jit(solution)/shard_map/ppermute | solution.py:18
  9.1 18.8 %collective-permute-start.1 = (bf16[3,1,1024]{2,0,1:T(4,128)(2,1)}, bf16[3,1,1024]{2,0,1:T(4,128)(2,1)}, u32[]{:S(2)}, u32[]{:S(2)}) collective-permute-start(bf16[3,1,1024]{2,0,1:T(4,128)(2,1)} %copy.41), channel_id=1, source_target_pairs={{1,0},{2,1},{3,2},{5,4},{6,5},{7,6},{9,8},{10,9},{11,10},{13,12},{... | collective-permute-start | bytes 18440 | tf_op jit(solution)/shard_map/ppermute | solution.py:19
  22.6 2.9 %copy-start.17 = (f32[3,1024]{1,0:T(4,128)S(1)}, f32[3,1024]{1,0:T(4,128)}, u32[]{:S(2)}) copy-start(f32[3,1024]{1,0:T(4,128)} %param.18) | copy-start | bytes 36868
  22.6 2.8 %copy-start.18 = (f32[3,1024]{1,0:T(4,128)S(1)}, f32[3,1024]{1,0:T(4,128)}, u32[]{:S(2)}) copy-start(f32[3,1024]{1,0:T(4,128)} %param.17) | copy-start | bytes 36868
  22.7 2.8 %copy-start.19 = (f32[3,1024]{1,0:T(4,128)S(1)}, f32[3,1024]{1,0:T(4,128)}, u32[]{:S(2)}) copy-start(f32[3,1024]{1,0:T(4,128)} %param.16) | copy-start | bytes 36868
  29.8 2.2 %copy-start.9 = (f32[3,1024]{1,0:T(4,128)S(1)}, f32[3,1024]{1,0:T(4,128)}, u32[]{:S(2)}) copy-start(f32[3,1024]{1,0:T(4,128)} %get-tuple-element.26) | copy-start | bytes 36868
  29.8 2.2 %copy-start.10 = (f32[3,1024]{1,0:T(4,128)S(1)}, f32[3,1024]{1,0:T(4,128)}, u32[]{:S(2)}) copy-start(f32[3,1024]{1,0:T(4,128)} %get-tuple-element.27) | copy-start | bytes 36868
  29.8 2.2 %copy-start.11 = (f32[3,1,1024]{2,0,1:T(4,128)S(1)}, f32[3,1,1024]{2,0,1:T(4,128)}, u32[]{:S(2)}) copy-start(f32[3,1,1024]{2,0,1:T(4,128)} %copy.82) | copy-start | bytes 36868
  34.4 1.1 %copy-start.1 = (f32[3,128,1024]{1,2,0:T(8,128)}, f32[3,128,1024]{1,2,0:T(8,128)S(1)}, u32[]{:S(2)}) copy-start(f32[3,128,1024]{1,2,0:T(8,128)S(1)} %fusion.24) | copy-start | bytes 4718596
  35.6 6.5 %copy-start.13 = (f32[8,8]{0,1:T(8,128)S(1)}, f32[8,8]{0,1:T(8,128)}, u32[]{:S(2)}) copy-start(f32[8,8]{0,1:T(8,128)} %get-tuple-element.32) | copy-start | bytes 772
  35.6 6.5 %copy-start.14 = (f32[8,8]{0,1:T(8,128)S(1)}, f32[8,8]{0,1:T(8,128)}, u32[]{:S(2)}) copy-start(f32[8,8]{0,1:T(8,128)} %get-tuple-element.33) | copy-start | bytes 772
  36.4 14.4 %all-to-all-start = ((f32[4,256,128]{2,1,0:T(8,128)}), f32[4,256,128]{2,1,0:T(8,128)S(1)}, u32[]{:S(2)}, u32[]{:S(2)}) async-start(f32[4,256,128]{2,1,0:T(8,128)} %bitcast.5), calls=%async_computation | async-start | bytes 1048576 | tf_op jit(solution)/shard_map/all_to_all | solution.py:102
  54.2 3.1 %copy-start.3 = (f32[256,128,16]{1,2,0:T(8,128)S(1)}, f32[256,128,16]{1,2,0:T(8,128)}, u32[]{:S(2)}) copy-start(f32[256,128,16]{1,2,0:T(8,128)} %fusion.7) | copy-start | bytes 6291460
  59.8 0.8 copy-start.7
  59.8 0.8 copy-start.8
  59.8 0.8 copy-start.15
  62.4 13.7 %copy-start.2 = (f32[3,128,1024]{1,2,0:T(8,128)S(1)}, f32[3,128,1024]{1,2,0:T(8,128)}, u32[]{:S(2)}) copy-start(f32[3,128,1024]{1,2,0:T(8,128)} %copy-done.1) | copy-start | bytes 4718596
  62.4 13.7 %copy-start.20 = (f32[1024]{0:T(1024)S(1)}, f32[1024]{0:T(1024)}, u32[]{:S(2)}) copy-start(f32[1024]{0:T(1024)} %param.24) | copy-start | bytes 12292
where the time goes:
time: 80.6 us; the launch traced here: 80 us
  matrix products  25.3 us (31%)
  local copies, waits for them, and re-layouts  19.1 us (24%)
  blocking collectives  12.3 us (15%)
  other arithmetic  10.4 us (13%)
  starting transfers between devices  9.83 us (12%)
  waiting for transfers between devices  2.68 us (3%)
    all_to_all x1, blocking collectives, body(): lax.all_to_all(convolved, 'col', split_axis=1, concat_axis=0, tiled=True)  12.3 us
    dot_general x2, matrix products, forward(): return jnp.einsum('cfk,kl->cfl', turned, second_block, precision=highest)  9.19 us
    unnamed x49, local copies, waits for them, and re-layouts  8.32 us
    all_to_all x1, starting transfers between devices, body(): lax.all_to_all(product.T, 'col', split_axis=0, concat_axis=1, tiled=True)  5.57 us
    dot_general x1, matrix products, body(): jnp.dot(mixed_rows, out_weight, preferred_element_type=jnp.float32)  3.73 us
    dot_general x2, matrix products, forward(): first = jnp.einsum('sfa,cab->cfsb', first_table, values, precision=highest)  3.72 us
    ppermute x1, starting transfers between devices, padded_2(): before = lax.ppermute(last, axis, up)  2.98 us
    all_to_all x1, waiting for transfers between devices, body(): lax.all_to_all(product.T, 'col', split_axis=0, concat_axis=1, tiled=True)  2.68 us
  transfers between devices with their start and end apart: 3, of which 1 were waited for; matrix products, arithmetic and copies ran while one was open for 30% of the time, Pallas kernels for 0%

commit v1 on v0

--- a/solution.py
+++ b/solution.py
@@ -1,8 +1,12 @@
+import functools
 import math
 
 import jax
 import jax.numpy as jnp
+import numpy as np
 from jax import lax
+from jax.experimental import pallas as pl
+from jax.experimental.pallas import tpu as pltpu
 from jax.sharding import PartitionSpec as P
 
 highest = lax.Precision.HIGHEST
@@ -70,7 +74,7 @@
     return result / span_len
 
 
-def body(
+def spread_body(
     gate_in,
     mult_in,
     value_in,
@@ -178,6 +182,410 @@
     ]
 
 
+f32, bf16 = (jnp.float32, jnp.bfloat16)
+EDGE = 16
+
+
+def wave_tables(seq_len):
+    odd = 2 * np.arange(seq_len, dtype=np.int64) + 1
+    angle = (odd[:, None] * odd[None, :] % (8 * seq_len)) * (math.pi / (4 * seq_len))
+    pieces = []
+    for table in (np.cos(angle), np.sin(angle)):
+        high = table.astype(bf16)
+        pieces += [high, (table - high.astype(np.float64)).astype(bf16)]
+    half = odd * (math.pi / (4 * seq_len))
+    turn = np.stack([np.cos(half), np.sin(half)]).astype(np.float32)
+    turn = np.repeat(turn[:, :, None], 128, axis=2)
+    return (np.stack(pieces), turn)
+
+
+def feature_table(seq_len, feature_count):
+    position = np.arange(seq_len, dtype=np.float64)
+    bands = (feature_count - 1) // 2
+    values = np.linspace(0.0001, bands - 1, bands)
+    angles = (2.0 * math.pi / seq_len * position)[:, None] * values[None, :]
+    tau = position / (seq_len - 1)
+    table = np.concatenate([tau[:, None], np.cos(angles), -np.sin(angles)], axis=1)
+    return np.pad(table, ((0, 0), (0, 128 - feature_count))).astype(np.float32)
+
+
+def sine(x):
+    turns = jnp.floor(x * (1.0 / math.pi) + 0.5)
+    r = x - turns * 3.140625
+    r = r - turns * 9.67502593994140625e-4
+    r = r - turns * 1.509957990978376432e-7
+    sign = 1.0 - 2.0 * (turns - 2.0 * jnp.floor(turns * 0.5))
+    s = r * r
+    poly = 1.0 / 362880.0 - s * (1.0 / 39916800.0)
+    poly = -1.0 / 5040.0 + s * poly
+    poly = 1.0 / 120.0 + s * poly
+    poly = -1.0 / 6.0 + s * poly
+    return sign * (r + r * s * poly)
+
+
+def split(value):
+    high = value.astype(bf16)
+    return (high, (value - high.astype(f32)).astype(bf16))
+
+
+def mul(a, b):
+    return jnp.dot(a, b, preferred_element_type=f32)
+
+
+def mul_precise(a, b):
+    return jnp.dot(a, b, preferred_element_type=f32, precision=highest)
+
+
+def neighbours(rows, before, after):
+    count = rows.shape[0]
+    index = lax.broadcasted_iota(jnp.int32, rows.shape, 0)
+    up = jnp.where(index == 0, before, pltpu.roll(rows, 1, 0))
+    down = jnp.where(index == count - 1, after, pltpu.roll(rows, count - 1, 0))
+    return (up, down)
+
+
+def short_form(rows, taps, before, after):
+    up, down = neighbours(rows, before, after)
+    return taps[0:1] * up + taps[1:2] * rows + taps[2:3] * down
+
+
+def conv_kernel(
+    n,
+    gate_hbm,
+    mult_hbm,
+    value_hbm,
+    taps_gate_hbm,
+    taps_mult_hbm,
+    taps_value_hbm,
+    first_hbm,
+    second_hbm,
+    ahead_hbm,
+    behind_hbm,
+    decay_hbm,
+    skip_hbm,
+    weight_hbm,
+    table_hbm,
+    turn_hbm,
+    feature_hbm,
+    out_ref,
+    gate,
+    mult,
+    value,
+    taps_gate,
+    taps_mult,
+    taps_value,
+    second_ref,
+    decay_ref,
+    skip_ref,
+    first,
+    ahead_w,
+    behind_w,
+    weight,
+    table,
+    turn,
+    feature,
+    sent,
+    came,
+    whole,
+    back_sent,
+    back_came,
+    halo_sent,
+    halo_came,
+    kernel_re,
+    kernel_im,
+    spec,
+    gate_part,
+    direct,
+    total,
+    load_sems,
+    send_sems,
+    recv_sems,
+    back_send,
+    back_recv,
+    halo_send,
+    halo_recv,
+):
+    me = lax.axis_index("col")
+    rows, channels = gate.shape
+    group = channels // n
+    seq_len = rows * n
+    near = me + 1 - 2 * lax.rem(me, 2)
+    peers = []
+    for j in range(1, n // 2):
+        peers += [lax.rem(me + 2 * j, n), lax.rem(near + 2 * j, n)]
+    peers.append(near)
+
+    def columns(owner):
+        return pl.ds(pl.multiple_of(owner * group, group), group)
+
+    loads = [
+        pltpu.make_async_copy(s, d, load_sems.at[i])
+        for i, (s, d) in enumerate(
+            [
+                (value_hbm.at[0], value),
+                (mult_hbm.at[0], mult),
+                (taps_value_hbm, taps_value),
+                (taps_mult_hbm, taps_mult),
+                (feature_hbm, feature),
+                (first_hbm, first.at[pl.ds(0, first_hbm.shape[0])]),
+                (second_hbm, second_ref),
+                (decay_hbm, decay_ref),
+                (ahead_hbm.at[:, columns(me)], ahead_w),
+                (behind_hbm.at[:, columns(me)], behind_w),
+                (table_hbm, table),
+                (turn_hbm, turn),
+                (gate_hbm.at[0], gate),
+                (taps_gate_hbm, taps_gate),
+                (skip_hbm, skip_ref),
+                (weight_hbm, weight),
+            ]
+        )
+    ]
+    for load in loads:
+        load.start()
+    barrier = pltpu.get_barrier_semaphore()
+    for peer in peers:
+        pl.semaphore_signal(
+            barrier, inc=1, device_id={"col": peer}, device_id_type=pl.DeviceIdType.MESH
+        )
+    for load in loads[:4]:
+        load.wait()
+
+    def pack(owner):
+        cols = columns(owner)
+        v = value[:, cols].astype(f32)
+        m = mult[:, cols].astype(f32)
+        zero = jnp.zeros((1, group), f32)
+        vs = short_form(v, taps_value[:, cols], zero, zero)
+        ms = short_form(m, taps_mult[:, cols], zero, zero)
+        sent[owner, pl.ds(0, rows), :] = (vs * ms).astype(bf16)
+        edges = jnp.concatenate(
+            [v[0:2], v[rows - 2 : rows], m[0:2], m[rows - 2 : rows], jnp.zeros((8, group), f32)], axis=0
+        )
+        sent[owner, pl.ds(rows, EDGE), :] = edges.astype(bf16)
+
+    def remote(src, dst, ssem, rsem, peer):
+        return pltpu.make_async_remote_copy(
+            src_ref=src,
+            dst_ref=dst,
+            send_sem=ssem,
+            recv_sem=rsem,
+            device_id={"col": peer},
+            device_id_type=pl.DeviceIdType.MESH,
+        )
+
+    copies = []
+    for i, peer in enumerate(peers):
+        pack(peer)
+        if i == 0:
+            pl.semaphore_wait(barrier, n - 1)
+        copy = remote(sent.at[peer], came.at[me], send_sems.at[peer], recv_sems.at[me], peer)
+        copy.start()
+        copies.append(copy)
+    loads[12].wait()
+    right, left = (lax.rem(me + 1, n), lax.rem(me + n - 1, n))
+    for side, (row, target) in enumerate([(rows - 1, right), (0, left)]):
+        base = rows - EDGE if row else 0
+        at = row - base
+        parts = [r[base : base + EDGE, :].astype(f32)[at : at + 1] for r in (gate, mult, value)]
+        tile = jnp.concatenate(parts + [jnp.zeros((EDGE - 3, channels), f32)], axis=0)
+        halo_sent[side] = tile.astype(bf16)
+        copy = remote(
+            halo_sent.at[side], halo_came.at[side], halo_send.at[side], halo_recv.at[side], target
+        )
+        copy.start()
+        copies.append(copy)
+    pack(me)
+
+    for load in loads[4:10]:
+        load.wait()
+    used = first_hbm.shape[0]
+    at = lax.broadcasted_iota(jnp.int32, first.shape, 0)
+    first_w = jnp.where(at < used, first[...], 0.0)
+    hidden = sine(mul_precise(feature[...], first_w))
+    hidden = sine(mul_precise(hidden, second_ref[...]))
+    later = pltpu.roll(hidden, seq_len - 1, 0)
+    rates = decay_ref[:, columns(me)]
+    index = lax.broadcasted_iota(jnp.int32, (seq_len, group), 0)
+    tau = index.astype(f32) * (1.0 / (seq_len - 1))
+    fade = jnp.exp(-rates * tau)
+    step = jnp.exp(-rates * (1.0 / (seq_len - 1)))
+    ahead = mul_precise(hidden, ahead_w[...]) * fade
+    behind = mul_precise(later, behind_w[...]) * (fade * step)
+    behind = jnp.where(index == seq_len - 1, 0.0, behind)
+    power = jnp.sum(ahead * ahead + behind * behind, axis=0, keepdims=True)
+    scale = lax.rsqrt(power + 1e-06) * (2.0 / (2 * seq_len))
+    loads[10].wait()
+    loads[11].wait()
+    high, low = split((ahead + behind) * scale)
+    even = mul(table[0], high) + mul(table[1], high) + mul(table[0], low)
+    high, low = split((ahead - behind) * scale)
+    odd = mul(table[2], high) + mul(table[3], high) + mul(table[2], low)
+    cos_half = turn[0][:, 0:1]
+    sin_half = turn[1][:, 0:1]
+    kernel_re[...] = cos_half * even + sin_half * odd
+    kernel_im[...] = sin_half * even - cos_half * odd
+
+    whole[pl.ds(pl.multiple_of(me * rows, rows), rows), :] = sent[me, pl.ds(0, rows), :]
+    came[me, pl.ds(rows, EDGE), :] = sent[me, pl.ds(rows, EDGE), :]
+    for peer in reversed(peers):
+        remote(sent.at[peer], came.at[peer], send_sems.at[peer], recv_sems.at[peer], peer).wait_recv()
+        whole[pl.ds(pl.multiple_of(peer * rows, rows), rows), :] = came[peer, pl.ds(0, rows), :]
+    edges = [came[s, pl.ds(rows, EDGE), :].astype(f32) for s in range(n)]
+    own_taps = [t[:, columns(me)] for t in (taps_value, taps_mult)]
+    tile_at = lax.broadcasted_iota(jnp.int32, (EDGE, group), 0)
+    for s in range(n):
+        top = bottom = 1.0
+        for k, taps in enumerate(own_taps):
+            e = edges[s][4 * k : 4 * k + 4]
+            first_row = taps[1:2] * e[0:1] + taps[2:3] * e[1:2]
+            last_row = taps[0:1] * e[2:3] + taps[1:2] * e[3:4]
+            if s > 0:
+                first_row += taps[0:1] * edges[s - 1][4 * k + 3 : 4 * k + 4]
+            if s < n - 1:
+                last_row += taps[2:3] * edges[s + 1][4 * k : 4 * k + 1]
+            top, bottom = (top * first_row, bottom * last_row)
+        for base, at, row in ((s * rows, 0, top), ((s + 1) * rows - EDGE, EDGE - 1, bottom)):
+            old = whole[base : base + EDGE, :].astype(f32)
+            whole[base : base + EDGE, :] = jnp.where(tile_at == at, row, old).astype(bf16)
+
+    x = whole[...]
+    xc = mul(table[0], x) + mul(table[1], x)
+    xs = mul(table[2], x) + mul(table[3], x)
+    kr, ki = (kernel_re[...], kernel_im[...])
+    spec[0], spec[1] = split(xc * kr + xs * ki)
+    spec[2], spec[3] = split(xs * kr - xc * ki)
+
+    def invert(owner):
+        take = pl.ds(pl.multiple_of(owner * rows, rows), rows)
+        ch, cl, sh, sl = (table[i, take, :] for i in range(4))
+        return (
+            mul(ch, spec[0]) + mul(sh, spec[2])
+            + mul(cl, spec[0]) + mul(sl, spec[2])
+            + mul(ch, spec[1]) + mul(sh, spec[3])
+        )
+
+    for peer in peers:
+        back_sent[peer] = invert(peer).astype(bf16)
+        copy = remote(
+            back_sent.at[peer], back_came.at[me], back_send.at[peer], back_recv.at[me], peer
+        )
+        copy.start()
+        copies.append(copy)
+    own_back = invert(me)
+
+    for side, target in enumerate((left, right)):
+        remote(
+            halo_sent.at[side], halo_came.at[side], halo_send.at[side], halo_recv.at[side], target
+        ).wait_recv()
+    loads[13].wait()
+    loads[14].wait()
+    has_left = (me > 0).astype(f32)
+    has_right = (me < n - 1).astype(f32)
+    for s in range(n):
+        cols = slice(s * group, (s + 1) * group)
+        before = halo_came[0, :, cols].astype(f32) * has_left
+        after = halo_came[1, :, cols].astype(f32) * has_right
+        parts = []
+        for i, (r, taps) in enumerate(((gate, taps_gate), (mult, taps_mult), (value, taps_value))):
+            parts.append(
+                short_form(r[:, cols].astype(f32), taps[:, cols], before[i : i + 1], after[i : i + 1])
+            )
+        gate_part[s] = parts[0]
+        direct[s] = skip_ref[:, cols] * (parts[1] * parts[2])
+    loads[15].wait()
+
+    def project(owner, convolved):
+        gated = ((convolved + direct[owner]) * gate_part[owner]).astype(bf16)
+        return mul(gated, weight[columns(owner), :])
+
+    total[...] = project(me, own_back)
+    for i, peer in enumerate(reversed(peers)):
+        remote(
+            back_sent.at[peer], back_came.at[peer], back_send.at[peer], back_recv.at[peer], peer
+        ).wait_recv()
+        term = project(peer, back_came[peer].astype(f32))
+        if i < n - 2:
+            total[...] += term
+        else:
+            out_ref[0] = (total[...] + term).astype(bf16)
+    for copy in copies:
+        copy.wait_send()
+
+
+def fused_body(n, *args):
+    gate_in, mult_in, value_in, tg, tm, tv, first, second, ahead, behind, decay, skip, weight = args
+    _, rows, channels = gate_in.shape
+    seq_len, group = (rows * n, channels // n)
+    width = weight.shape[1]
+    tables, turn = wave_tables(seq_len)
+    features = feature_table(seq_len, first.shape[0])
+    vmem = pl.BlockSpec(memory_space=pltpu.VMEM)
+    main = pl.BlockSpec(memory_space=pltpu.HBM)
+    hidden_count = second.shape[0]
+    dma = pltpu.SemaphoreType.DMA
+    return pl.pallas_call(
+        functools.partial(conv_kernel, n),
+        out_shape=jax.ShapeDtypeStruct((1, rows, width), bf16),
+        in_specs=[main] * 16,
+        out_specs=vmem,
+        scratch_shapes=[
+            pltpu.VMEM((rows, channels), bf16),
+            pltpu.VMEM((rows, channels), bf16),
+            pltpu.VMEM((rows, channels), bf16),
+            pltpu.VMEM(tg.shape, f32),
+            pltpu.VMEM(tm.shape, f32),
+            pltpu.VMEM(tv.shape, f32),
+            pltpu.VMEM(second.shape, f32),
+            pltpu.VMEM((1, channels), f32),
+            pltpu.VMEM((1, channels), f32),
+            pltpu.VMEM((128, hidden_count), f32),
+            pltpu.VMEM((hidden_count, group), f32),
+            pltpu.VMEM((hidden_count, group), f32),
+            pltpu.VMEM(weight.shape, bf16),
+            pltpu.VMEM(tables.shape, bf16),
+            pltpu.VMEM(turn.shape, f32),
+            pltpu.VMEM(features.shape, f32),
+            pltpu.VMEM((n, rows + EDGE, group), bf16),
+            pltpu.VMEM((n, rows + EDGE, group), bf16),
+            pltpu.VMEM((seq_len, group), bf16),
+            pltpu.VMEM((n, rows, group), bf16),
+            pltpu.VMEM((n, rows, group), bf16),
+            pltpu.VMEM((2, EDGE, channels), bf16),
+            pltpu.VMEM((2, EDGE, channels), bf16),
+            pltpu.VMEM((seq_len, group), f32),
+            pltpu.VMEM((seq_len, group), f32),
+            pltpu.VMEM((4, seq_len, group), bf16),
+            pltpu.VMEM((n, rows, group), f32),
+            pltpu.VMEM((n, rows, group), f32),
+            pltpu.VMEM((rows, width), f32),
+            dma((16,)),
+            dma((n,)),
+            dma((n,)),
+            dma((n,)),
+            dma((n,)),
+            dma((2,)),
+            dma((2,)),
+        ],
+        compiler_params=pltpu.CompilerParams(
+            collective_id=0, has_side_effects=True
+        ),
+    )(
+        gate_in, mult_in, value_in, tg, tm, tv, first, second, ahead, behind,
+        decay.reshape(1, channels), skip.reshape(1, channels), weight,
+        jnp.asarray(tables), jnp.asarray(turn), jnp.asarray(features),
+    )
+
+
+def body_for(n, *args):
+    _, rows, channels = args[0].shape
+    small = rows * n <= 1024 and rows % 128 == 0 and channels % (128 * n) == 0
+    network = args[6].shape[0] <= 128 and args[6].shape[1] == 128
+    if n >= 2 and n % 2 == 0 and small and network and args[3].shape[0] == 3:
+        return fused_body(n, *args)
+    return spread_body(*args)
+
+
 def solution(mesh):
     in_specs = (
         P(("grp", "row"), "col", None),
@@ -195,4 +603,6 @@
         P(),
     )
     out_specs = P(("grp", "row"), "col", None)
+
+    body = functools.partial(body_for, mesh.shape["col"])
     return jax.shard_map(body, mesh=mesh, in_specs=in_specs, out_specs=out_specs, check_vma=False)

time: 80.6 us -> 18 us (0.22)
  matrix products: 25.3 us -> 0 us
  local copies, waits for them, and re-layouts: 19.1 us -> 1.88 us
  Pallas kernels: 0 us -> 16 us
  blocking collectives: 12.3 us -> 0 us
  other arithmetic: 10.4 us -> 0 us
  starting transfers between devices: 9.83 us -> 0 us
  waiting for transfers between devices: 2.68 us -> 0 us
    dot_general x11 -> x0, matrix products: 25.3 us -> none  [the longest x2 9.19 us: forward(): return jnp.einsum('cfk,kl->cfl', turned, second_block, precision=highest)]
    pallas_call x0 -> x1, Pallas kernels: none -> 16 us  [fused_body(): pl.pallas_call(functools.partial(conv_kernel, n), out_shape=jax.ShapeDtyp...]
    all_to_all x1 -> x0, blocking collectives: 12.3 us -> none  [body(): lax.all_to_all(convolved, 'col', split_axis=1, concat_axis=0, tiled=True)]
    unnamed x49 -> x1, local copies, waits for them, and re-layouts: 8.32 us -> 1.88 us
    all_to_all x1 -> x0, starting transfers between devices: 5.57 us -> none  [body(): lax.all_to_all(product.T, 'col', split_axis=0, concat_axis=1, tiled=True)]
    ppermute x2 -> x0, starting transfers between devices: 4.26 us -> none  [the longest x1 2.98 us: padded_2(): before = lax.ppermute(last, axis, up)]
    slice x6 -> x0, local copies, waits for them, and re-layouts: 3.38 us -> none  [the longest x3 1.74 us: swap_halves(): stacked[..., width:]]
    ppermute x2 -> x0, local copies, waits for them, and re-layouts: 3.04 us -> none  [the longest x1 1.93 us: padded_2(): after = lax.ppermute(leading, axis, down)]
  transfers between devices with their start and end apart: 3 -> 0, of which waited for: 1 -> 0; matrix products, arithmetic and copies ran while one was open for 30% -> 0% of each run, Pallas kernels for 0% -> 0%
where the time goes in v1:
time: 18 us; the launch traced here: 17.9 us
  Pallas kernels  16 us (89%)
  local copies, waits for them, and re-layouts  1.88 us (10%)
    pallas_call x1, Pallas kernels, fused_body(): pl.pallas_call(functools.partial(conv_kernel, n), out_shape=jax.ShapeDtyp...  16 us
    unnamed x1, local copies, waits for them, and re-layouts  1.88 us

profile of v1, /device:TPU:0, one launch (start us, length us, event | category | flops | bytes accessed | tf_op | source)
XLA Modules:
  0.0 17.9 jit_solution(6226262794238550154)
XLA Ops:
  0.0 16.0 %shard_map.154 = bf16[1,128,2048]{2,1,0:T(8,128)(2,1)} custom-call(bf16[1,128,1024]{2,1,0:T(8,128)(2,1)} %gate_hbm.1, bf16[1,128,1024]{2,1,0:T(8,128)(2,1)} %mult_hbm.1, bf16[1,128,1024]{2,1,0:T(8,128)(2,1)} %value_hbm.1, f32[3,1024]{1,0:T(4,128)} %taps_gate_hbm.1, f32[3,1024]{1,0:T(4,128)} %taps_mult_hbm.1, f32[3,1024]{1,0:T(4,128)} %taps_value_hbm.1, ...), custom_call_target="tpu_custom_call" | custom-call | tf_op jit(solution)/shard_map/pallas_call | solution.py:527
  16.0 1.9 %copy.18 = bf16[1,128,2048]{2,1,0:T(8,128)(2,1)} copy(bf16[1,128,2048]{2,1,0:T(8,128)(2,1)} %shard_map.154) | data formatting | bytes 1048576

commit v2 on v1

--- a/solution.py
+++ b/solution.py
@@ -184,6 +184,7 @@
 
 f32, bf16 = (jnp.float32, jnp.bfloat16)
 EDGE = 16
+PARTS = 2
 
 
 def wave_tables(seq_len):
@@ -351,18 +352,23 @@
     for load in loads[:4]:
         load.wait()
 
-    def pack(owner):
-        cols = columns(owner)
+    part = group // PARTS
+
+    def piece(owner, h):
+        return pl.ds(pl.multiple_of(owner * group + h * part, part), part)
+
+    def pack(owner, h):
+        cols = piece(owner, h)
         v = value[:, cols].astype(f32)
         m = mult[:, cols].astype(f32)
-        zero = jnp.zeros((1, group), f32)
+        zero = jnp.zeros((1, part), f32)
         vs = short_form(v, taps_value[:, cols], zero, zero)
         ms = short_form(m, taps_mult[:, cols], zero, zero)
-        sent[owner, pl.ds(0, rows), :] = (vs * ms).astype(bf16)
+        sent[h, owner, pl.ds(0, rows), :] = (vs * ms).astype(bf16)
         edges = jnp.concatenate(
-            [v[0:2], v[rows - 2 : rows], m[0:2], m[rows - 2 : rows], jnp.zeros((8, group), f32)], axis=0
+            [v[0:2], v[rows - 2 : rows], m[0:2], m[rows - 2 : rows], jnp.zeros((8, part), f32)], axis=0
         )
-        sent[owner, pl.ds(rows, EDGE), :] = edges.astype(bf16)
+        sent[h, owner, pl.ds(rows, EDGE), :] = edges.astype(bf16)
 
     def remote(src, dst, ssem, rsem, peer):
         return pltpu.make_async_remote_copy(
@@ -375,13 +381,16 @@
         )
 
     copies = []
-    for i, peer in enumerate(peers):
-        pack(peer)
-        if i == 0:
-            pl.semaphore_wait(barrier, n - 1)
-        copy = remote(sent.at[peer], came.at[me], send_sems.at[peer], recv_sems.at[me], peer)
-        copy.start()
-        copies.append(copy)
+    for h in range(PARTS):
+        for i, peer in enumerate(peers):
+            pack(peer, h)
+            if i + h == 0:
+                pl.semaphore_wait(barrier, n - 1)
+            copy = remote(
+                sent.at[h, peer], came.at[h, me], send_sems.at[h, peer], recv_sems.at[h, me], peer
+            )
+            copy.start()
+            copies.append(copy)
     loads[12].wait()
     right, left = (lax.rem(me + 1, n), lax.rem(me + n - 1, n))
     for side, (row, target) in enumerate([(rows - 1, right), (0, left)]):
@@ -395,7 +404,8 @@
         )
         copy.start()
         copies.append(copy)
-    pack(me)
+    for h in range(PARTS):
+        pack(me, h)
 
     for load in loads[4:10]:
         load.wait()
@@ -426,53 +436,65 @@
     kernel_re[...] = cos_half * even + sin_half * odd
     kernel_im[...] = sin_half * even - cos_half * odd
 
-    whole[pl.ds(pl.multiple_of(me * rows, rows), rows), :] = sent[me, pl.ds(0, rows), :]
-    came[me, pl.ds(rows, EDGE), :] = sent[me, pl.ds(rows, EDGE), :]
-    for peer in reversed(peers):
-        remote(sent.at[peer], came.at[peer], send_sems.at[peer], recv_sems.at[peer], peer).wait_recv()
-        whole[pl.ds(pl.multiple_of(peer * rows, rows), rows), :] = came[peer, pl.ds(0, rows), :]
-    edges = [came[s, pl.ds(rows, EDGE), :].astype(f32) for s in range(n)]
-    own_taps = [t[:, columns(me)] for t in (taps_value, taps_mult)]
-    tile_at = lax.broadcasted_iota(jnp.int32, (EDGE, group), 0)
-    for s in range(n):
-        top = bottom = 1.0
-        for k, taps in enumerate(own_taps):
-            e = edges[s][4 * k : 4 * k + 4]
-            first_row = taps[1:2] * e[0:1] + taps[2:3] * e[1:2]
-            last_row = taps[0:1] * e[2:3] + taps[1:2] * e[3:4]
-            if s > 0:
-                first_row += taps[0:1] * edges[s - 1][4 * k + 3 : 4 * k + 4]
-            if s < n - 1:
-                last_row += taps[2:3] * edges[s + 1][4 * k : 4 * k + 1]
-            top, bottom = (top * first_row, bottom * last_row)
-        for base, at, row in ((s * rows, 0, top), ((s + 1) * rows - EDGE, EDGE - 1, bottom)):
-            old = whole[base : base + EDGE, :].astype(f32)
-            whole[base : base + EDGE, :] = jnp.where(tile_at == at, row, old).astype(bf16)
-
-    x = whole[...]
-    xc = mul(table[0], x) + mul(table[1], x)
-    xs = mul(table[2], x) + mul(table[3], x)
-    kr, ki = (kernel_re[...], kernel_im[...])
-    spec[0], spec[1] = split(xc * kr + xs * ki)
-    spec[2], spec[3] = split(xs * kr - xc * ki)
-
-    def invert(owner):
+
+    def near_product(h):
+        whole[h, pl.ds(pl.multiple_of(me * rows, rows), rows), :] = sent[h, me, pl.ds(0, rows), :]
+        came[h, me, pl.ds(rows, EDGE), :] = sent[h, me, pl.ds(rows, EDGE), :]
+        for peer in reversed(peers):
+            remote(
+                sent.at[h, peer], came.at[h, peer], send_sems.at[h, peer], recv_sems.at[h, peer], peer
+            ).wait_recv()
+            whole[h, pl.ds(pl.multiple_of(peer * rows, rows), rows), :] = came[
+                h, peer, pl.ds(0, rows), :
+            ]
+        edges = [came[h, s, pl.ds(rows, EDGE), :].astype(f32) for s in range(n)]
+        own_taps = [t[:, piece(me, h)] for t in (taps_value, taps_mult)]
+        tile_at = lax.broadcasted_iota(jnp.int32, (EDGE, part), 0)
+        for s in range(n):
+            top = bottom = 1.0
+            for k, taps in enumerate(own_taps):
+                e = edges[s][4 * k : 4 * k + 4]
+                first_row = taps[1:2] * e[0:1] + taps[2:3] * e[1:2]
+                last_row = taps[0:1] * e[2:3] + taps[1:2] * e[3:4]
+                if s > 0:
+                    first_row += taps[0:1] * edges[s - 1][4 * k + 3 : 4 * k + 4]
+                if s < n - 1:
+                    last_row += taps[2:3] * edges[s + 1][4 * k : 4 * k + 1]
+                top, bottom = (top * first_row, bottom * last_row)
+            for base, at, row in ((s * rows, 0, top), ((s + 1) * rows - EDGE, EDGE - 1, bottom)):
+                old = whole[h, base : base + EDGE, :].astype(f32)
+                whole[h, base : base + EDGE, :] = jnp.where(tile_at == at, row, old).astype(bf16)
+
+    def invert(owner, h):
         take = pl.ds(pl.multiple_of(owner * rows, rows), rows)
         ch, cl, sh, sl = (table[i, take, :] for i in range(4))
         return (
-            mul(ch, spec[0]) + mul(sh, spec[2])
-            + mul(cl, spec[0]) + mul(sl, spec[2])
-            + mul(ch, spec[1]) + mul(sh, spec[3])
+            mul(ch, spec[h, 0]) + mul(sh, spec[h, 2])
+            + mul(cl, spec[h, 0]) + mul(sl, spec[h, 2])
+            + mul(ch, spec[h, 1]) + mul(sh, spec[h, 3])
         )
 
-    for peer in peers:
-        back_sent[peer] = invert(peer).astype(bf16)
-        copy = remote(
-            back_sent.at[peer], back_came.at[me], back_send.at[peer], back_recv.at[me], peer
-        )
-        copy.start()
-        copies.append(copy)
-    own_back = invert(me)
+    for h in range(PARTS):
+        near_product(h)
+        x = whole[h]
+        xc = mul(table[0], x) + mul(table[1], x)
+        xs = mul(table[2], x) + mul(table[3], x)
+        cols = slice(h * part, (h + 1) * part)
+        kr, ki = (kernel_re[:, cols], kernel_im[:, cols])
+        spec[h, 0], spec[h, 1] = split(xc * kr + xs * ki)
+        spec[h, 2], spec[h, 3] = split(xs * kr - xc * ki)
+        for peer in peers:
+            back_sent[h, peer] = invert(peer, h).astype(bf16)
+            copy = remote(
+                back_sent.at[h, peer],
+                back_came.at[h, me],
+                back_send.at[h, peer],
+                back_recv.at[h, me],
+                peer,
+            )
+            copy.start()
+            copies.append(copy)
+    own_back = jnp.concatenate([invert(me, h) for h in range(PARTS)], axis=1)
 
     for side, target in enumerate((left, right)):
         remote(
@@ -501,10 +523,16 @@
 
     total[...] = project(me, own_back)
     for i, peer in enumerate(reversed(peers)):
-        remote(
-            back_sent.at[peer], back_came.at[peer], back_send.at[peer], back_recv.at[peer], peer
-        ).wait_recv()
-        term = project(peer, back_came[peer].astype(f32))
+        for h in range(PARTS):
+            remote(
+                back_sent.at[h, peer],
+                back_came.at[h, peer],
+                back_send.at[h, peer],
+                back_recv.at[h, peer],
+                peer,
+            ).wait_recv()
+        arrived = [back_came[h, peer].astype(f32) for h in range(PARTS)]
+        term = project(peer, jnp.concatenate(arrived, axis=1))
         if i < n - 2:
             total[...] += term
         else:
@@ -518,6 +546,7 @@
     _, rows, channels = gate_in.shape
     seq_len, group = (rows * n, channels // n)
     width = weight.shape[1]
+    part = group // PARTS
     tables, turn = wave_tables(seq_len)
     features = feature_table(seq_len, first.shape[0])
     vmem = pl.BlockSpec(memory_space=pltpu.VMEM)
@@ -526,7 +555,7 @@
     dma = pltpu.SemaphoreType.DMA
     return pl.pallas_call(
         functools.partial(conv_kernel, n),
-        out_shape=jax.ShapeDtypeStruct((1, rows, width), bf16),
+        out_shape=pltpu.VMEM((1, rows, width), bf16),
         in_specs=[main] * 16,
         out_specs=vmem,
         scratch_shapes=[
@@ -546,29 +575,29 @@
             pltpu.VMEM(tables.shape, bf16),
             pltpu.VMEM(turn.shape, f32),
             pltpu.VMEM(features.shape, f32),
-            pltpu.VMEM((n, rows + EDGE, group), bf16),
-            pltpu.VMEM((n, rows + EDGE, group), bf16),
-            pltpu.VMEM((seq_len, group), bf16),
-            pltpu.VMEM((n, rows, group), bf16),
-            pltpu.VMEM((n, rows, group), bf16),
+            pltpu.VMEM((PARTS, n, rows + EDGE, part), bf16),
+            pltpu.VMEM((PARTS, n, rows + EDGE, part), bf16),
+            pltpu.VMEM((PARTS, seq_len, part), bf16),
+            pltpu.VMEM((PARTS, n, rows, part), bf16),
+            pltpu.VMEM((PARTS, n, rows, part), bf16),
             pltpu.VMEM((2, EDGE, channels), bf16),
             pltpu.VMEM((2, EDGE, channels), bf16),
             pltpu.VMEM((seq_len, group), f32),
             pltpu.VMEM((seq_len, group), f32),
-            pltpu.VMEM((4, seq_len, group), bf16),
+            pltpu.VMEM((PARTS, 4, seq_len, part), bf16),
             pltpu.VMEM((n, rows, group), f32),
             pltpu.VMEM((n, rows, group), f32),
             pltpu.VMEM((rows, width), f32),
             dma((16,)),
-            dma((n,)),
-            dma((n,)),
-            dma((n,)),
-            dma((n,)),
+            dma((PARTS, n)),
+            dma((PARTS, n)),
+            dma((PARTS, n)),
+            dma((PARTS, n)),
             dma((2,)),
             dma((2,)),
         ],
         compiler_params=pltpu.CompilerParams(
-            collective_id=0, has_side_effects=True
+            collective_id=0, has_side_effects=True, vmem_limit_bytes=61 * 1024 * 1024
         ),
     )(
         gate_in, mult_in, value_in, tg, tm, tv, first, second, ahead, behind,
@@ -579,7 +608,7 @@
 
 def body_for(n, *args):
     _, rows, channels = args[0].shape
-    small = rows * n <= 1024 and rows % 128 == 0 and channels % (128 * n) == 0
+    small = rows * n <= 1024 and rows % 128 == 0 and channels % (128 * PARTS * n) == 0
     network = args[6].shape[0] <= 128 and args[6].shape[1] == 128
     if n >= 2 and n % 2 == 0 and small and network and args[3].shape[0] == 3:
         return fused_body(n, *args)

time: 18 us -> 15.2 us (0.84)
  Pallas kernels: 16 us -> 14.3 us
  local copies, waits for them, and re-layouts: 1.88 us -> 0.8 us
    pallas_call x1, Pallas kernels: 16 us -> 14.3 us  [fused_body(): pl.pallas_call(functools.partial(conv_kernel, n), out_shape=pltpu.VMEM((1...]
    unnamed x1, local copies, waits for them, and re-layouts: 1.88 us -> 0.8 us
where the time goes in v2:
time: 15.2 us; the launch traced here: 15.1 us
  Pallas kernels  14.3 us (94%)
  local copies, waits for them, and re-layouts  0.8 us (5%)
    pallas_call x1, Pallas kernels, fused_body(): pl.pallas_call(functools.partial(conv_kernel, n), out_shape=pltpu.VMEM((1...  14.3 us
    unnamed x1, local copies, waits for them, and re-layouts  0.8 us

profile of v2, /device:TPU:0, one launch (start us, length us, event | category | flops | bytes accessed | tf_op | source)
XLA Modules:
  0.0 15.1 jit_solution(15113977907061531001)
XLA Ops:
  0.0 14.3 %shard_map.154 = bf16[1,128,2048]{2,1,0:T(8,128)(2,1)S(1)} custom-call(bf16[1,128,1024]{2,1,0:T(8,128)(2,1)} %gate_hbm.1, bf16[1,128,1024]{2,1,0:T(8,128)(2,1)} %mult_hbm.1, bf16[1,128,1024]{2,1,0:T(8,128)(2,1)} %value_hbm.1, f32[3,1024]{1,0:T(4,128)} %taps_gate_hbm.1, f32[3,1024]{1,0:T(4,128)} %taps_mult_hbm.1, f32[3,1024]{1,0:T(4,128)} %taps_value_hbm.1, ...), custom_call_target="tpu_custom_call" | custom-call | tf_op jit(solution)/shard_map/pallas_call | solution.py:556
  14.3 0.8 %copy.18 = bf16[1,128,2048]{2,1,0:T(8,128)(2,1)} copy(bf16[1,128,2048]{2,1,0:T(8,128)(2,1)S(1)} %shard_map.154) | data formatting | bytes 1048576
